TPU v7x, 256 devices: a 4x2x16 block of a 4x16x16 slice. The times are simulated.
256 devices in a mesh: grp: 2 (over y), ep: 32 (over z, core), tp: 4 (over x).
Axes of the slice: x: 4, y: 2, z: 16, core: 2. Of those that a mesh axis runs over, the one named last changes fastest.
The devices are a block of a 4x16x16 slice.
Arguments:
- queries: bfloat16 [8192, 1024], P(('grp', 'ep'), 'tp'), parts along dimension 0, may hold values from -6 to 6
- context_lookup_vectors: bfloat16 [8192, 1024], P(('grp', 'ep'), 'tp'), parts along dimension 0, may hold values from -6 to 6
- values: bfloat16 [8192, 1024], P(('grp', 'ep'), 'tp'), parts along dimension 0, may hold values from -6 to 6
- key_shift: bfloat16 [8192, 8], P(('grp', 'ep'), 'tp'), parts along dimension 0, may hold values from -12 to 0
- head_gain: float32 [1024], P('tp'), may hold values from 0.1 to 1.9
- moe_rows: bfloat16 [32768, 2048], P(('grp', 'ep', 'tp')), parts along dimension 0, may hold values from -6 to 6
- routes: int32 [32768, 2], P(('grp', 'ep', 'tp')), parts along dimension 0, may hold values from 0 to 31, all different within a row; in each aligned block of 128 rows (0 to 127, 128 to 255, ...) at most 9 rows name the same one
- route_scores: float32 [32768, 2], P(('grp', 'ep', 'tp')), parts along dimension 0, may hold values from -8 to 8
- norm_gain: float32 [2048], replicated, may hold values from 0.1 to 1.9
- w_gate: bfloat16 [32, 2048, 3584], P('ep', None, 'tp'), may hold values from -0.125 to 0.125
- w_up: bfloat16 [32, 2048, 3584], P('ep', None, 'tp'), may hold values from -0.125 to 0.125
- w_down: bfloat16 [32, 3584, 2048], P('ep', 'tp'), may hold values from -0.09375 to 0.09375
Outputs:
- attn_out: bfloat16 [8192, 1024], P(('grp', 'ep'), 'tp'), parts along dimension 0
- moe_out: bfloat16 [32768, 2048], P(('grp', 'ep', 'tp')), parts along dimension 0
There are 2 independent parts, one for each index of `grp`. A program takes and returns all parts, laid end to end along the dimension named above; an argument that names none is the same for every part. Nothing has to cross between parts.
Inputs may be any that keep to these rules, and one draw needn't show every extreme that they name: `routes`: each row names 2 different experts. In the rows of one device no expert is named more than 9 times, and some device names some expert exactly 9 times.
All inputs are finite; a program needn't handle non-finite values.
Results may differ from a plain program's by a relative error of at most 0.013.
Values may be sent and summed in bfloat16 or wider, within the bound.
No kernel may reach another device: no remote copies, remote signals or barrier semaphores. Data moves between devices by JAX's collectives and lax.ppermute only.
A program may use at most 128 MiB of HBM per device.

v0:
```python
import math

import jax
import jax.numpy as jnp
from jax import lax
from jax.sharding import Mesh
from jax.sharding import PartitionSpec as P

EP = ("ep_0", "ep_1")
GRP_EP = ("grp", "ep_0", "ep_1")
GRP_EP_TP = ("grp", "ep_0", "ep_1", "tp")


EPS = 1e-06


def sent_together(arrays, axis, dim, along):
    widths = [a.shape[along] for a in arrays]
    both = jnp.concatenate(arrays, axis=along)
    filled = lax.all_gather(both, axis, axis=dim, tiled=True)
    return tuple(jnp.split(filled, [sum(widths[:k]) for k in range(1, len(widths))], axis=along))


def in_blocks(value, dim, peers):
    before, after = (value.shape[:dim], value.shape[dim + 1 :])
    return jnp.moveaxis(value.reshape(*before, peers, -1, *after), dim, 0)


def sent_and_summed(value, axis, dim):
    peers = lax.axis_size(axis)
    blocks = lax.all_to_all(in_blocks(value, dim, peers), axis, 0, 0, tiled=True)
    return jnp.sum(blocks.astype(jnp.float32), axis=0)


def laid_out(blocks, dim):
    blocks = jnp.moveaxis(blocks, 0, dim)
    shape = blocks.shape
    return blocks.reshape(*shape[:dim], shape[dim] * shape[dim + 1], *shape[dim + 2 :])


def turned_blocks(blocks, axes, order):
    shape = [lax.axis_size(a) for a in axes]
    blocks = blocks.reshape(*shape, *blocks.shape[1:])
    for k in order:
        blocks = lax.all_to_all(blocks, axes[k], split_axis=k, concat_axis=k, tiled=True)
    return blocks.reshape(-1, *blocks.shape[len(axes) :])


def core_and_chips(value, groups, order, split_dim, concat_dim):
    peers = lax.axis_size(groups[0]) * lax.axis_size(groups[1])
    blocks = in_blocks(value, split_dim, peers)
    return laid_out(turned_blocks(blocks, groups, order), concat_dim)


def exchange_in_groups(value, axis, split_dim, concat_dim, work, item_dim, out_dim):

    def moved(group):
        return lax.all_to_all(group, axis, split_axis=split_dim, concat_axis=concat_dim, tiled=True)

    items = jax.tree.leaves(value)[0].shape[item_dim]
    ends = [items * k // 2 for k in range(2 + 1)] if items % 2 == 0 else [0, items]
    groups = [
        jax.tree.map(lambda a: lax.slice_in_dim(a, low, high, axis=item_dim), value)
        for low, high in zip(ends, ends[1:])
    ]
    arrived = [moved(group) for group in groups]
    made = [work(group) for group in arrived]
    return jax.tree.map(lambda *parts: jnp.concatenate(parts, axis=out_dim), *made)


def all_weights(queries_local, all_keys, all_shift, query_start):
    count = all_keys.shape[0]
    heads = queries_local.shape[1]
    keys_local = all_keys.reshape(count, heads, -1)
    scale = 1.0 / math.sqrt(keys_local.shape[2])
    score = (
        jnp.einsum("thd,shd->hts", queries_local, keys_local, preferred_element_type=jnp.float32)
        * scale
    )
    score = score + all_shift.astype(jnp.float32).T[:, None, :]
    key_pos = jnp.arange(count, dtype=jnp.int32)
    query_pos = query_start + jnp.arange(queries_local.shape[0], dtype=jnp.int32)
    causal = key_pos[None, :] < query_pos[:, None]
    log_stay = jnp.where(causal, -jax.nn.softplus(score), 0.0)
    inner = lax.cumsum(log_stay, axis=2, reverse=True) - log_stay
    weight = jnp.where(causal, jnp.exp(jax.nn.log_sigmoid(score) + inner), 0.0)
    return weight.astype(jnp.bfloat16)


def mixer(queries, context_lookup_vectors, values, key_shift, head_gain):
    rows = queries.shape[0]
    heads = key_shift.shape[1]
    queries_local = queries.reshape(rows, heads, -1)
    query_start = lax.axis_index(EP) * rows
    all_keys, all_values, all_shift = sent_together(
        (context_lookup_vectors, values, key_shift), EP, 0, 1
    )
    weight = all_weights(queries_local, all_keys, all_shift, query_start)
    values_local = all_values.reshape(all_values.shape[0], heads, -1)
    mixed = jnp.einsum("hts,shd->thd", weight, values_local, preferred_element_type=jnp.float32)
    factor = lax.rsqrt(jnp.mean(mixed * mixed, axis=2, keepdims=True) + EPS)
    normed = mixed * factor * head_gain.reshape(heads, -1)
    return normed.reshape(rows, -1).astype(jnp.bfloat16)


def experts(moe_rows, routes, route_scores, norm_gain, w_gate, w_up, w_down):
    rows, width = moe_rows.shape
    top = routes.shape[1]
    ep_size = lax.axis_size(EP)
    capacity = top * rows // ep_size + max(1, top * rows // (8 * ep_size))
    rows_f = moe_rows.astype(jnp.float32)
    factor = lax.rsqrt(jnp.mean(rows_f * rows_f, axis=1, keepdims=True) + EPS)
    normed = (rows_f * factor * norm_gain).astype(jnp.bfloat16)
    route_weight = jax.nn.softmax(route_scores, axis=-1)
    flat = routes.reshape(-1)
    onehot = (flat[:, None] == jnp.arange(ep_size, dtype=jnp.int32)[None, :]).astype(jnp.int32)
    rank = jnp.sum((jnp.cumsum(onehot, axis=0) - onehot) * onehot, axis=1)
    slot_id = flat * capacity + rank
    slot_ids = jnp.arange(ep_size * capacity, dtype=jnp.int32)
    placing = jnp.any(
        slot_id.reshape(rows, top)[None, :, :] == slot_ids[:, None, None], axis=2
    ).astype(jnp.bfloat16)
    outgoing = jnp.dot(placing, normed, preferred_element_type=jnp.float32).astype(jnp.bfloat16)
    outgoing = outgoing.reshape(ep_size, capacity, width)
    gate_w = w_gate[0]
    up_w = w_up[0]
    down_w = w_down[0]

    def reduce_return(hidden, items):
        part = lax.slice_in_dim(hidden, 0, ep_size * items * lax.axis_size("tp"), axis=0)
        summed = sent_and_summed(
            jnp.dot(part, down_w, preferred_element_type=jnp.float32).astype(jnp.bfloat16), "tp", 0
        )
        result = summed.astype(jnp.bfloat16).reshape(ep_size, items, width)
        return core_and_chips(result, ("ep_0", "ep_1"), (1, 0), 0, 0)

    def hidden_rows(piece):
        gate = jnp.dot(piece, gate_w, preferred_element_type=jnp.float32)
        up = jnp.dot(piece, up_w, preferred_element_type=jnp.float32)
        return (jax.nn.silu(gate) * up).astype(jnp.bfloat16)

    def at_expert(received):
        items = received.shape[1]
        flat_rows = received.reshape(ep_size * items, width)
        hidden = hidden_rows(lax.all_gather(flat_rows, "tp", axis=0, tiled=True))
        return reduce_return(hidden, items)

    returned = exchange_in_groups(outgoing, EP, 0, 0, at_expert, 1, 1)
    returned = returned.reshape(ep_size * capacity, width)
    picked = returned[slot_id].reshape(rows, top, width).astype(jnp.float32)
    return jnp.sum(route_weight[:, :, None] * picked, axis=1).astype(jnp.bfloat16)


def local(
    queries,
    context_lookup_vectors,
    values,
    key_shift,
    head_gain,
    moe_rows,
    routes,
    route_scores,
    norm_gain,
    w_gate,
    w_up,
    w_down,
):
    attn_out = mixer(queries, context_lookup_vectors, values, key_shift, head_gain)
    moe_out = experts(moe_rows, routes, route_scores, norm_gain, w_gate, w_up, w_down)
    return (attn_out, moe_out)


def solution(mesh):
    torus = Mesh(
        mesh.devices.reshape(mesh.shape["grp"], 16, 2, mesh.shape["tp"]),
        ("grp", "ep_0", "ep_1", "tp"),
    )
    return jax.shard_map(
        local,
        mesh=torus,
        in_specs=(
            P(GRP_EP, "tp"),
            P(GRP_EP, "tp"),
            P(GRP_EP, "tp"),
            P(GRP_EP, "tp"),
            P("tp"),
            P(GRP_EP_TP, None),
            P(GRP_EP_TP, None),
            P(GRP_EP_TP, None),
            P(),
            P(EP, None, "tp"),
            P(EP, None, "tp"),
            P(EP, "tp", None),
        ),
        out_specs=(P(GRP_EP, "tp"), P(GRP_EP_TP, None)),
        check_vma=False,
    )
```

profile of v0, /device:TPU:38, one launch (start us, length us, event | category | flops | bytes accessed | tf_op | source)
XLA Modules:
  0.0 372.2 jit_solution(9929334086890800888)
XLA Ops:
  7.2 0.0 copy-start
  7.2 0.1 all-gather.5.cloned.1.call-start
  7.3 0.8 copy.61
  8.0 0.1 eq.38
  8.2 0.1 eq.42
  8.3 0.6 reduce-window.16
  8.9 0.2 slice_reduce_fusion
  9.2 0.1 fusion.29
  9.3 0.1 reduce_sum.64
  9.4 0.1 copy.65
  9.5 0.1 fusion.24
  9.6 1.2 fusion.18
  10.8 1.6 convolution_convert_fusion.1
  12.4 0.5 reshape.121
  12.9 0.0 copy-start.4
  12.9 0.0 copy-start.5
  12.9 0.0 copy-start.8
  13.0 125.0 %all_to_all.20 = bf16[32,9,2048]{2,1,0:T(8,128)(2,1)} all-to-all(bf16[32,9,2048]{2,1,0:T(8,128)(2,1)S(1)} %reshape.121), channel_id=1, replica_groups=mesh['grp'=2,'ep_0'=16,'ep_1'=2,'tp'=4] {'ep_0','ep_1'}, dimensions={0} | all-to-all | bytes 2359296 | tf_op jit(solution)/shard_map/all_to_all | solution.py:58
  138.0 2.6 reshape.122
  140.6 0.1 all-gather.5.cloned.1.call-update
  140.6 0.1 all-gather.3.cloned.1.call-start
  140.7 0.1 copy.54
  140.8 0.0 copy-done.5
  140.9 0.1 copy.53
  141.0 0.7 pad_maximum_fusion
  141.6 0.1 all-gather.3.cloned.1.call-update
  141.7 48.3 %all-gather.5.cloned.1.call-done = bf16[1152,2048]{1,0:T(8,128)(2,1)} async-done(((bf16[288,2048]{1,0:T(8,128)(2,1)}), bf16[1152,2048]{1,0:T(8,128)(2,1)}) %all-gather.5.cloned.1.call-update) | async-done | bytes 4718608 | tf_op jit(solution)/shard_map/all_gather | solution.py:145
  190.0 8.1 %fusion.13 = f32[1152,896]{1,0:T(8,128)S(1)} fusion(bf16[1152,2048]{1,0:T(8,128)(2,1)} %all-gather.5.cloned.1.call-done, bf16[1,2048,896]{2,1,0:T(8,128)(2,1)} %param.21), kind=kOutput, calls=%fused_computation.20 | convolution fusion | flops 4227858432 | bytes 12517376 | tf_op jit(solution)/shard_map/dot_general | solution.py:138
  198.1 0.0 copy-start.11
  198.2 5.3 %fusion.15 = bf16[1152,896]{1,0:T(8,128)(2,1)S(1)} fusion(bf16[1152,2048]{1,0:T(8,128)(2,1)S(1)} %copy-done.9, bf16[1,2048,896]{2,1,0:T(8,128)(2,1)S(1)} %copy-done.10, f32[1152,896]{1,0:T(8,128)S(1)} %fusion.13), kind=kOutput, calls=%fused_computation.22 | convolution fusion | flops 4234051584 | bytes 14581760 | tf_op jit(solution)/shard_map/dot_general | solution.py:139
  203.5 0.0 copy-done.11
  203.5 6.7 %convolution_convert_fusion = bf16[1152,2048]{1,0:T(8,128)(2,1)} fusion(bf16[1152,896]{1,0:T(8,128)(2,1)S(1)} %fusion.15, bf16[1,896,2048]{2,1,0:T(8,128)(2,1)S(1)} %copy-done.11), kind=kOutput, calls=%fused_computation.3 | convolution fusion | flops 4230217728 | bytes 10452992 | tf_op jit(solution)/shard_map/dot_general | solution.py:132
  210.2 7.3 %all-to-all-start.1 = ((bf16[4,288,2048]{2,1,0:T(8,128)(2,1)}), bf16[4,288,2048]{2,1,0:T(8,128)(2,1)}, u32[]{:S(2)}, u32[]{:S(2)}) async-start(bf16[4,288,2048]{2,1,0:T(8,128)(2,1)} %bitcast.69), calls=%async_computation.1 | async-start | bytes 9437184 | tf_op jit(solution)/shard_map/all_to_all | solution.py:31
  217.5 0.1 mul.110
  217.7 0.1 copy.60
  217.9 1.1 iota_compare_fusion
  219.0 53.3 %all-gather.3.cloned.1.call-done = bf16[4096,514]{0,1:T(8,128)(2,1)} async-done(((bf16[128,514]{0,1:T(8,128)(2,1)}), bf16[4096,514]{0,1:T(8,128)(2,1)}) %all-gather.3.cloned.1.call-update) | async-done | bytes 4210704 | tf_op jit(solution)/shard_map/all_gather | solution.py:20
  272.3 3.9 %fusion.34 = (bf16[4096,256]{0,1:T(8,128)(2,1)}, bf16[4096,256]{0,1:T(8,128)(2,1)S(1)}) fusion(bf16[4096,514]{0,1:T(8,128)(2,1)} %all-gather.3.cloned.1.call-done), kind=kLoop, calls=%fused_computation.63 | loop fusion | bytes 8388608 | tf_op jit(solution)/shard_map/split | solution.py:21
  276.2 0.0 all-to-all-done.1
  276.2 3.3 reduce_sum.66
  279.5 1.6 reshape_reshape_reshape.6
  281.1 2.3 copy.66
  283.4 0.0 copy-start.3
  283.5 5.0 %all_to_all.21 = bf16[16,2,1,9,2048]{4,0,3,2,1:T(8,128)(2,1)S(1)} all-to-all(bf16[16,2,1,9,2048]{4,0,3,2,1:T(8,128)(2,1)S(1)} %copy.66), channel_id=1, replica_groups=mesh['grp'=2,'ep_0'=16,'ep_1'=2,'tp'=4] {'ep_1'}, dimensions={1} | all-to-all | bytes 2359296 | tf_op jit(solution)/shard_map/all_to_all | solution.py:45
  288.5 2.3 copy.67
  290.8 8.2 %all-to-all-start.3 = ((bf16[16,2,1,9,2048]{4,1,3,2,0:T(2,128)(2,1)}), bf16[16,2,1,9,2048]{4,1,3,2,0:T(2,128)(2,1)}, u32[]{:S(2)}, u32[]{:S(2)}) async-start(bf16[16,2,1,9,2048]{4,1,3,2,0:T(2,128)(2,1)} %copy.67), calls=%async_computation.3 | async-start | bytes 2359296 | tf_op jit(solution)/shard_map/all_to_all | solution.py:45
  299.0 0.9 convert_bitcast_fusion
  299.9 6.3 %fusion.8 = (f32[2,128,4096]{1,2,0:T(8,128)S(1)}, f32[2,128,4096]{1,2,0:T(8,128)}) fusion(pred[128,4096]{0,1:T(8,128)(4,1)S(1)} %copy-done.3, f32[2,4096]{1,0:T(2,128)S(1)} %convert_bitcast_fusion, bf16[4096,2,128]{0,2,1:T(8,128)(2,1)} %bitcast.71, bf16[128,256]{1,0:T(8,128)(2,1)S(1)} %copy-done), kind=kOutput, calls=%fused_computation.14 | convolution fusion | flops 278921216 | bytes 11108352 | tf_op jit(solution)/shard_map/thd,shd->hts/dot_general | solution.py:77
  306.2 10.1 %fusion.9 = f32[2,128,32,128]{1,2,3,0:T(8,128)S(1)} fusion(f32[2,128,32,128]{1,3,2,0:T(8,128)S(1)} %bitcast.70), kind=kOutput, calls=%fused_computation.16 | output fusion | flops 133169152 | bytes 8388608 | tf_op jit(solution)/shard_map/reduce-window
  316.3 2.0 copy-done.1
  318.3 0.2 reduce-window.15
  318.5 2.7 broadcast_add_fusion
  321.2 2.4 copy.58
  323.6 6.4 %fusion.6 = bf16[2,128,4096]{1,2,0:T(8,128)(2,1)S(1)} fusion(f32[2,128,32,128]{1,3,2,0:T(8,128)S(1)} %copy.58, f32[2,128,4096]{1,2,0:T(8,128)S(1)} %copy-done.2, pred[128,4096]{0,1:T(8,128)(4,1)S(1)} %copy-done.3), kind=kLoop, calls=%fused_computation.12 | loop fusion | flops 20971520 | bytes 11010048 | tf_op jit(solution)/shard_map/convert_element_type | solution.py:87
  330.0 0.0 copy-start.7
  330.0 0.8 multiply_reduce_fusion.1
  330.8 0.1 multiply_convert_fusion
  330.9 0.7 copy.69
  331.7 22.5 %all-to-all-done.3 = bf16[16,2,1,9,2048]{4,1,3,2,0:T(2,128)(2,1)} async-done(((bf16[16,2,1,9,2048]{4,1,3,2,0:T(2,128)(2,1)}), bf16[16,2,1,9,2048]{4,1,3,2,0:T(2,128)(2,1)}, u32[]{:S(2)}, u32[]{:S(2)}) %all-to-all-start.3) | async-done | bytes 1179680 | tf_op jit(solution)/shard_map/all_to_all | solution.py:45
  354.2 1.9 copy.68
  356.1 0.6 reshape_reshape_reshape.7
  356.7 2.3 gather_fusion
  359.0 2.4 reshape.124
  361.4 3.9 %multiply_reduce_fusion = bf16[128,2048]{1,0:T(8,128)(2,1)} fusion(f32[128,2,2048]{2,1,0:T(2,128)S(1)} %reshape.124, f32[128,2]{1,0:T(8,128)S(1)} %copy.60), kind=kLoop, calls=%fused_computation.24 | loop fusion | flops 786432 | bytes 2622464 | tf_op jit(solution)/shard_map/reduce_sum | solution.py:151
  (28 shorter events, 0.2 us)
Async XLA Ops:
  7.2 292.7 %copy-start = (bf16[128,256]{1,0:T(8,128)(2,1)S(1)}, bf16[128,256]{1,0:T(8,128)(2,1)}, u32[]{:S(2)}) copy-start(bf16[128,256]{1,0:T(8,128)(2,1)} %param.12) | copy-start | bytes 196612
  7.2 182.8 %all-gather.5.cloned.1.call-start = ((), (), s32[]{:S(2)}) async-start(), calls=%async_computation.5 | async-start | bytes 5898240 | tf_op jit(solution)/shard_map/all_gather | solution.py:145
  12.9 127.8 %copy-start.4 = (bf16[128,256]{1,0:T(8,128)(2,1)S(1)}, bf16[128,256]{1,0:T(8,128)(2,1)}, u32[]{:S(2)}) copy-start(bf16[128,256]{1,0:T(8,128)(2,1)} %param.14) | copy-start | bytes 196612
  12.9 127.9 %copy-start.5 = (bf16[128,256]{1,0:T(8,128)(2,1)S(1)}, bf16[128,256]{1,0:T(8,128)(2,1)}, u32[]{:S(2)}) copy-start(bf16[128,256]{1,0:T(8,128)(2,1)} %param.13) | copy-start | bytes 196612
  12.9 128.0 %copy-start.8 = (bf16[128,2]{0,1:T(2,128)(2,1)S(1)}, bf16[128,2]{0,1:T(2,128)(2,1)}, u32[]{:S(2)}) copy-start(bf16[128,2]{0,1:T(2,128)(2,1)} %param.15) | copy-start | bytes 1540
  140.6 131.6 %all-gather.3.cloned.1.call-start = ((), (), s32[]{:S(2)}) async-start(), calls=%async_computation.4 | async-start | bytes 4392960 | tf_op jit(solution)/shard_map/all_gather | solution.py:20
  190.0 8.1 %copy-start.9 = (bf16[1152,2048]{1,0:T(8,128)(2,1)S(1)}, bf16[1152,2048]{1,0:T(8,128)(2,1)}, u32[]{:S(2)}) copy-start(bf16[1152,2048]{1,0:T(8,128)(2,1)} %all-gather.5.cloned.1.call-done) | copy-start | bytes 14155780
  190.0 8.1 %copy-start.10 = (bf16[1,2048,896]{2,1,0:T(8,128)(2,1)S(1)}, bf16[1,2048,896]{2,1,0:T(8,128)(2,1)}, u32[]{:S(2)}) copy-start(bf16[1,2048,896]{2,1,0:T(8,128)(2,1)} %param.22) | copy-start | bytes 11010052
  198.1 5.3 %copy-start.11 = (bf16[1,896,2048]{2,1,0:T(8,128)(2,1)S(1)}, bf16[1,896,2048]{2,1,0:T(8,128)(2,1)}, u32[]{:S(2)}) copy-start(bf16[1,896,2048]{2,1,0:T(8,128)(2,1)} %param.23) | copy-start | bytes 11010052
  210.2 7.5 %copy-start.6 = (f32[128,2]{0,1:T(2,128)S(1)}, f32[128,2]{0,1:T(2,128)}, u32[]{:S(2)}) copy-start(f32[128,2]{0,1:T(2,128)} %param.19) | copy-start | bytes 3076
  210.2 66.0 %all-to-all-start.1 = ((bf16[4,288,2048]{2,1,0:T(8,128)(2,1)}), bf16[4,288,2048]{2,1,0:T(8,128)(2,1)}, u32[]{:S(2)}, u32[]{:S(2)}) async-start(bf16[4,288,2048]{2,1,0:T(8,128)(2,1)} %bitcast.69), calls=%async_computation.1 | async-start | bytes 9437184 | tf_op jit(solution)/shard_map/all_to_all | solution.py:31
  283.4 16.4 %copy-start.3 = (pred[128,4096]{0,1:T(8,128)(4,1)S(1)}, pred[128,4096]{0,1:T(8,128)(4,1)}, u32[]{:S(2)}) copy-start(pred[128,4096]{0,1:T(8,128)(4,1)} %iota_compare_fusion) | copy-start | bytes 1572868
  290.8 63.4 %all-to-all-start.3 = ((bf16[16,2,1,9,2048]{4,1,3,2,0:T(2,128)(2,1)}), bf16[16,2,1,9,2048]{4,1,3,2,0:T(2,128)(2,1)}, u32[]{:S(2)}, u32[]{:S(2)}) async-start(bf16[16,2,1,9,2048]{4,1,3,2,0:T(2,128)(2,1)} %copy.67), calls=%async_computation.3 | async-start | bytes 2359296 | tf_op jit(solution)/shard_map/all_to_all | solution.py:45
  316.3 2.0 copy-start.1
  321.2 2.4 copy-start.2
  330.0 0.8 copy-start.7
Sparse Core Ops, SparseCore 0:
  140.8 49.1 all-gather.4
  191.8 80.4 all-gather.2
where the time goes:
time: 373 us; the launch traced here: 372 us
  blocking collectives  130 us (35%)
  waiting for transfers between devices  124 us (33%)
  other arithmetic  31.5 us (8%)
  matrix products  28.8 us (8%)
  local copies, waits for them, and re-layouts  27.6 us (7%)
  starting transfers between devices  15.7 us (4%)
  between operations  14.4 us (4%)
    all_to_all x1, blocking collectives, moved(): lax.all_to_all(group, axis, split_axis=split_dim, concat_axis=concat_dim,...  125 us
    all_gather x1, waiting for transfers between devices, sent_together(): filled = lax.all_gather(both, axis, axis=dim, tiled=True)  53.3 us
    all_gather x1, waiting for transfers between devices, at_expert(): hidden = hidden_rows(lax.all_gather(flat_rows, 'tp', axis=0, tiled=True))  48.3 us
    all_to_all x1, waiting for transfers between devices, turned_blocks(): lax.all_to_all(blocks, axes[k], split_axis=k, concat_axis=k, tiled=True)  22.5 us
    another operation x4, other arithmetic  10.9 us
    all_to_all x1, starting transfers between devices, turned_blocks(): lax.all_to_all(blocks, axes[k], split_axis=k, concat_axis=k, tiled=True)  8.24 us
    dot_general x1, matrix products, hidden_rows(): gate = jnp.dot(piece, gate_w, preferred_element_type=jnp.float32)  8.11 us
  transfers between devices with their start and end apart: 4, of which 3 were waited for; matrix products, arithmetic and copies ran while one was open for 15% of the time, Pallas kernels for 0%

commit v1 on v0

v1 whole, which is shorter than its diff:
```python
import functools
import math

import jax
import jax.numpy as jnp
from jax import lax
from jax.experimental import pallas as pl
from jax.experimental.pallas import tpu as pltpu
from jax.sharding import Mesh
from jax.sharding import PartitionSpec as P


EP = ("ep_0", "ep_1")
GRP_EP = ("grp", "ep_0", "ep_1")
GRP_EP_TP = ("grp", "ep_0", "ep_1", "tp")
EPS = 1e-06
LANES = 128
SUB = 16


def shifted(value, axis, step):
    size = lax.axis_size(axis)
    return lax.ppermute(value, axis, [(i, (i + step) % size) for i in range(size)])


def attention_kernel(where_ref, q_ref, kv_ref, gain_ref, out_ref, *, heads, group):
    index = where_ref[0]
    rows = q_ref.shape[0]
    size = LANES
    scale = 1.0 / math.sqrt(size)
    row_id = lax.broadcasted_iota(jnp.int32, (rows, size), 0)
    lane_id = lax.broadcasted_iota(jnp.int32, (rows, size), 1)
    later = (
        lax.broadcasted_iota(jnp.int32, (size, size), 0)
        > lax.broadcasted_iota(jnp.int32, (size, size), 1)
    ).astype(jnp.bfloat16)
    last = index // group
    contract_last = (((1,), (1,)), ((), ()))

    def step(i, carry):
        first = (last - i) * group
        sums = [carry[2 * h] for h in range(heads)]
        tails = [carry[2 * h + 1] for h in range(heads)]
        for h in range(heads):
            q = q_ref[:, h * size : (h + 1) * size]
            for j in reversed(range(group)):
                b = first + j
                k = kv_ref[b, h * size : (h + 1) * size, :]
                v = kv_ref[b, (heads + h) * size : (heads + h + 1) * size, :]
                shift = kv_ref[b, 2 * heads * size : 2 * heads * size + 8, :].astype(jnp.float32)
                shift = shift[h : h + 1, :]
                score = (
                    lax.dot_general(q, k, contract_last, preferred_element_type=jnp.float32)
                    * scale
                    + shift
                )
                causal = lane_id + (b - index) * size < row_id
                soft = jnp.log1p(jnp.exp(-jnp.abs(score)))
                log_stay = jnp.where(causal, -(jnp.maximum(score, 0.0) + soft), 0.0)
                high = log_stay.astype(jnp.bfloat16)
                low = (log_stay - high.astype(jnp.float32)).astype(jnp.bfloat16)
                inner = jnp.dot(high, later, preferred_element_type=jnp.float32) + jnp.dot(
                    low, later, preferred_element_type=jnp.float32
                )
                log_take = jnp.minimum(score, 0.0) - soft
                weight = jnp.where(causal, jnp.exp(log_take + inner + tails[h]), 0.0)
                sums[h] = sums[h] + jnp.dot(
                    weight.astype(jnp.bfloat16), v, preferred_element_type=jnp.float32
                )
                tails[h] = tails[h] + jnp.sum(log_stay, axis=1, keepdims=True)
        out = []
        for h in range(heads):
            out += [sums[h], tails[h]]
        return tuple(out)

    start = []
    for _ in range(heads):
        start += [jnp.zeros((rows, size), jnp.float32), jnp.zeros((rows, 1), jnp.float32)]
    final = lax.fori_loop(0, last + 1, step, tuple(start))
    for h in range(heads):
        mixed = final[2 * h]
        factor = lax.rsqrt(jnp.mean(mixed * mixed, axis=1, keepdims=True) + EPS)
        gain = gain_ref[:, h * size : (h + 1) * size]
        out_ref[:, h * size : (h + 1) * size] = (mixed * factor * gain).astype(out_ref.dtype)


def packed_context(context_lookup_vectors, values, key_shift):
    heads = key_shift.shape[1]
    parts = [context_lookup_vectors[:, h * LANES : (h + 1) * LANES] for h in range(heads)]
    parts += [values[:, h * LANES : (h + 1) * LANES] for h in range(heads)]
    parts.append(jnp.pad(key_shift.T, ((0, 8 - heads), (0, 0))))
    return jnp.concatenate(parts, axis=0)


def mixer(queries, gathered, head_gain, heads):
    rows, width = queries.shape
    where = lax.axis_index(EP).astype(jnp.int32).reshape(1)
    blocks = lax.axis_size(EP)
    vmem = pl.BlockSpec(memory_space=pltpu.VMEM)
    return pl.pallas_call(
        functools.partial(attention_kernel, heads=heads, group=4),
        out_shape=jax.ShapeDtypeStruct((rows, width), jnp.bfloat16),
        in_specs=[pl.BlockSpec(memory_space=pltpu.SMEM), vmem, vmem, vmem],
        out_specs=vmem,
        compiler_params=pltpu.CompilerParams(vmem_limit_bytes=16 * 1024 * 1024),
        name="mixer",
        cost_estimate=pl.CostEstimate(
            flops=8 * rows * rows * blocks * width,
            bytes_accessed=2 * gathered.size,
            transcendentals=3 * rows * rows * blocks * heads,
        ),
    )(where, queries, gathered.reshape(blocks, -1, LANES), head_gain.reshape(1, width))


def feed_kernel(*refs, count, steps, sizes):
    rows = refs[:count]
    gate_ref, up_ref, down_ref = refs[count : count + 3]
    outs = refs[count + 3 : count + 3 + len(sizes)]
    gate_sum, up_sum, hidden = refs[count + 3 + len(sizes) :]
    i = pl.program_id(0)

    @pl.when(i < steps)
    def _():
        piece = jnp.concatenate([r[...] for r in rows], axis=0) if count > 1 else rows[0][...]
        gate = jnp.dot(piece, gate_ref[0], preferred_element_type=jnp.float32)
        up = jnp.dot(piece, up_ref[0], preferred_element_type=jnp.float32)

        @pl.when(i == 0)
        def _():
            gate_sum[...] = gate
            up_sum[...] = up

        @pl.when((i > 0) & (i < steps - 1))
        def _():
            gate_sum[...] += gate
            up_sum[...] += up

        @pl.when(i == steps - 1)
        def _():
            g = gate_sum[...] + gate
            hidden[...] = (g / (1.0 + jnp.exp(-g)) * (up_sum[...] + up)).astype(hidden.dtype)

    @pl.when(i >= steps)
    def _():
        made = jnp.dot(hidden[...], down_ref[0], preferred_element_type=jnp.float32)
        low = 0
        for out, size in zip(outs, sizes):
            out[...] = made[low : low + size].astype(out.dtype)
            low += size


def feed(pieces, sizes, w_gate, w_up, w_down, steps=4):
    width, units = w_gate.shape[1:]
    counts = tuple(p.shape[0] for p in pieces)
    total = sum(counts)
    count = len(pieces)
    part = width // steps
    return pl.pallas_call(
        functools.partial(feed_kernel, count=count, steps=steps, sizes=sizes),
        grid=(2 * steps,),
        out_shape=[jax.ShapeDtypeStruct((n, width), jnp.bfloat16) for n in sizes],
        in_specs=[pl.BlockSpec((n, part), lambda i: (0, jnp.minimum(i, steps - 1))) for n in counts]
        + [pl.BlockSpec((1, part, units), lambda i: (0, jnp.minimum(i, steps - 1), 0))] * 2
        + [pl.BlockSpec((1, units, part), lambda i: (0, 0, jnp.maximum(i - steps, 0)))],
        out_specs=[
            pl.BlockSpec((n, part), lambda i: (0, jnp.maximum(i - steps, 0))) for n in sizes
        ],
        scratch_shapes=[
            pltpu.VMEM((total, units), jnp.float32),
            pltpu.VMEM((total, units), jnp.float32),
            pltpu.VMEM((total, units), jnp.bfloat16),
        ],
        compiler_params=pltpu.CompilerParams(
            dimension_semantics=("arbitrary",), vmem_limit_bytes=20 * 1024 * 1024
        ),
        name="feed",
        cost_estimate=pl.CostEstimate(
            flops=6 * total * width * units,
            bytes_accessed=6 * width * units + 4 * total * width,
            transcendentals=total * units,
        ),
    )(*pieces, w_gate, w_up, w_down)


def join_kernel(own_ref, a_ref, b_ref, c_ref, d_ref, out_ref, tiles_ref):
    half, _ = a_ref.shape
    for low, first, second in ((0, a_ref, c_ref), (half, b_ref, d_ref)):
        for k in range(SUB):
            cut = slice(k * LANES, (k + 1) * LANES)
            value = (
                own_ref[low : low + half, cut].astype(jnp.float32)
                + first[:, cut].astype(jnp.float32)
                + second[:, cut].astype(jnp.float32)
            )
            tiles_ref[pl.ds(low * SUB + k, half, stride=SUB), :] = value
    out_ref[...] = tiles_ref[...].astype(out_ref.dtype)


def joined(own, before_low, before_high, after_low, after_high):
    count, width = own.shape
    vmem = pl.BlockSpec(memory_space=pltpu.VMEM)
    return pl.pallas_call(
        join_kernel,
        out_shape=jax.ShapeDtypeStruct((count * SUB, LANES), jnp.bfloat16),
        in_specs=[vmem] * 5,
        out_specs=vmem,
        scratch_shapes=[pltpu.VMEM((count * SUB, LANES), jnp.float32)],
        compiler_params=pltpu.CompilerParams(vmem_limit_bytes=12 * 1024 * 1024),
        name="join",
        cost_estimate=pl.CostEstimate(
            flops=1000 * count * width, bytes_accessed=8 * count * width, transcendentals=0
        ),
    )(own, before_low, before_high, after_low, after_high)


def added(*arrays):
    total = arrays[0].astype(jnp.float32)
    for a in arrays[1:]:
        total = total + a.astype(jnp.float32)
    return total.astype(jnp.bfloat16)


def at_experts(own, w_gate, w_up, w_down):
    half = own.shape[0] // 2
    before = shifted(own, "tp", 1)
    after = shifted(own, "tp", -1)
    across_low = shifted(before[:half], "tp", 1)
    across_high = shifted(after[half:], "tp", -1)
    own_part, before_low, before_high, after_low, after_high = feed(
        (own, before, after), (2 * half, half, half, half, half), w_gate, w_up, w_down
    )
    from_before_high = shifted(after_high, "tp", 1)
    from_after_low = shifted(before_low, "tp", -1)
    across_low, across_high, own_part = lax.optimization_barrier(
        (across_low, across_high, own_part)
    )
    low, high = feed((across_low, across_high), (half, half), w_gate, w_up, w_down)
    low = shifted(low, "tp", 1)
    high = shifted(high, "tp", -1)
    from_before_low = shifted(added(after_low, low), "tp", 1)
    from_after_high = shifted(added(before_high, high), "tp", -1)
    return joined(own_part, from_before_low, from_before_high, from_after_low, from_after_high)


def exchanged(tiles, peers):
    tiles = tiles.reshape(peers, -1, SUB, LANES)
    return lax.all_to_all(tiles, EP, 0, 0, tiled=True)


def local(
    queries,
    context_lookup_vectors,
    values,
    key_shift,
    head_gain,
    moe_rows,
    routes,
    route_scores,
    norm_gain,
    w_gate,
    w_up,
    w_down,
):
    rows, width = moe_rows.shape
    top = routes.shape[1]
    heads = key_shift.shape[1]
    peers = lax.axis_size(EP)
    capacity = top * rows // peers + max(1, top * rows // (8 * peers))
    first = (capacity + 1) // 2
    chunks = (first, capacity - first)
    rows_f = moe_rows.astype(jnp.float32)
    factor = lax.rsqrt(jnp.mean(rows_f * rows_f, axis=1, keepdims=True) + EPS)
    normed = (rows_f * factor * norm_gain).astype(jnp.bfloat16)
    route_weight = jax.nn.softmax(route_scores, axis=-1)
    flat = routes.reshape(-1)
    onehot = (flat[:, None] == jnp.arange(peers, dtype=jnp.int32)[None, :]).astype(jnp.int32)
    rank = jnp.sum((jnp.cumsum(onehot, axis=0) - onehot) * onehot, axis=1)
    sent = []
    weights = []
    low = 0
    for size in chunks:
        slot = jnp.where(
            (rank >= low) & (rank < low + size), flat * size + rank - low, -1
        ).reshape(rows, top)
        slots = jnp.arange(peers * size, dtype=jnp.int32)
        placing = jnp.any(slot[None, :, :] == slots[:, None, None], axis=2).astype(jnp.bfloat16)
        sent.append(
            jnp.dot(placing, normed, preferred_element_type=jnp.float32).astype(jnp.bfloat16)
        )
        weights.append(
            jnp.sum(
                jnp.where(slot[:, :, None] == slots[None, None, :], route_weight[:, :, None], 0.0),
                axis=1,
            )
        )
        low += size

    arrived = []
    for s, size in zip(sent, chunks):
        arrived.append(exchanged(s, peers).reshape(peers * size, width))
    context = packed_context(context_lookup_vectors, values, key_shift)
    _, context = lax.optimization_barrier((arrived[0], context))
    gathered = lax.all_gather(context, EP, axis=0, tiled=True)
    attn_out = mixer(queries, gathered, head_gain, heads)
    total = jnp.zeros((rows, width), jnp.float32)
    for a, w, size in zip(arrived, weights, chunks):
        result = at_experts(a, w_gate, w_up, w_down)
        back = exchanged(result, peers).reshape(peers * size, width)
        high = w.astype(jnp.bfloat16)
        rest = (w - high.astype(jnp.float32)).astype(jnp.bfloat16)
        total = (
            total
            + jnp.dot(high, back, preferred_element_type=jnp.float32)
            + jnp.dot(rest, back, preferred_element_type=jnp.float32)
        )
    return (attn_out, total.astype(jnp.bfloat16))


def solution(mesh):
    cores = 2
    chips = mesh.shape["ep"] // cores
    torus = Mesh(
        mesh.devices.reshape(mesh.shape["grp"], chips, cores, mesh.shape["tp"]),
        ("grp", "ep_0", "ep_1", "tp"),
    )
    return jax.shard_map(
        local,
        mesh=torus,
        in_specs=(
            P(GRP_EP, "tp"),
            P(GRP_EP, "tp"),
            P(GRP_EP, "tp"),
            P(GRP_EP, "tp"),
            P("tp"),
            P(GRP_EP_TP, None),
            P(GRP_EP_TP, None),
            P(GRP_EP_TP, None),
            P(),
            P(EP, None, "tp"),
            P(EP, None, "tp"),
            P(EP, "tp", None),
        ),
        out_specs=(P(GRP_EP, "tp"), P(GRP_EP_TP, None)),
        check_vma=False,
    )
```

time: 373 us -> 274 us (0.73); the launches traced: 372 us -> 269 us
  blocking collectives: 130 us -> 0 us
  starting transfers between devices: 15.7 us -> 81.2 us
  Pallas kernels: 0 us -> 32.4 us
  other arithmetic: 31.5 us -> 3.22 us
  matrix products: 28.8 us -> 3.87 us
  local copies, waits for them, and re-layouts: 27.6 us -> 18.4 us
  waiting for transfers between devices: 124 us -> 115 us
    all_to_all x2 -> x0, blocking collectives: 130 us -> none  [the longest x1 125 us: moved(): lax.all_to_all(group, axis, split_axis=split_dim, concat_axis=concat_dim,...]
    all_gather x2 -> x1, waiting for transfers between devices: 102 us -> 0.01 us  [local(): gathered = lax.all_gather(context, EP, axis=0, tiled=True)]
    all_to_all x2 -> x4, waiting for transfers between devices: 22.5 us -> 70.7 us  [exchanged(): return lax.all_to_all(tiles, EP, 0, 0, tiled=True)]
    ppermute x0 -> x20, waiting for transfers between devices: none -> 44.3 us  [shifted(): lax.ppermute(value, axis, [(i, (i + step) % size) for i in range(size)])]
    ppermute x0 -> x20, starting transfers between devices: none -> 33.5 us  [shifted(): lax.ppermute(value, axis, [(i, (i + step) % size) for i in range(size)])]
    pallas_call x0 -> x7, Pallas kernels: none -> 32.4 us  [the longest x4 26.9 us: feed(): pl.pallas_call(functools.partial(feed_kernel, count=count, steps=steps, s...]
    all_to_all x2 -> x4, starting transfers between devices: 15.6 us -> 47.6 us  [exchanged(): return lax.all_to_all(tiles, EP, 0, 0, tiled=True)]
    dot_general x6, matrix products: 28.8 us -> 3.87 us  [the longest x2 1.83 us: local(): jnp.dot(placing, normed, preferred_element_type=jnp.float32)]
  transfers between devices with their start and end apart: 4 -> 25, of which waited for: 3 -> 12; matrix products, arithmetic and copies ran while one was open for 15% -> 2% of each run, Pallas kernels for 0% -> 11%
where the time goes in v1:
time: 274 us; the launch traced here: 269 us
  waiting for transfers between devices  115 us (42%)
  starting transfers between devices  81.2 us (30%)
  Pallas kernels  32.4 us (12%)
  local copies, waits for them, and re-layouts  18.4 us (7%)
  between operations  14.5 us (5%)
  matrix products  3.87 us (1%)
  other arithmetic  3.22 us (1%)
    all_to_all x4, waiting for transfers between devices, exchanged(): return lax.all_to_all(tiles, EP, 0, 0, tiled=True)  70.7 us
    all_to_all x4, starting transfers between devices, exchanged(): return lax.all_to_all(tiles, EP, 0, 0, tiled=True)  47.6 us
    ppermute x20, waiting for transfers between devices, shifted(): lax.ppermute(value, axis, [(i, (i + step) % size) for i in range(size)])  44.3 us
    ppermute x20, starting transfers between devices, shifted(): lax.ppermute(value, axis, [(i, (i + step) % size) for i in range(size)])  33.5 us
    pallas_call x4, Pallas kernels, feed(): pl.pallas_call(functools.partial(feed_kernel, count=count, steps=steps, s...  26.9 us
    unnamed x47, local copies, waits for them, and re-layouts  17.6 us
  transfers between devices with their start and end apart: 25, of which 12 were waited for; matrix products, arithmetic and copies ran while one was open for 2% of the time, Pallas kernels for 11%

profile of v1, /device:TPU:38, one launch (start us, length us, event | category | flops | bytes accessed | tf_op | source)
XLA Modules:
  0.0 268.5 jit_solution(17826816132428869887)
XLA Ops:
  7.2 0.8 copy.40
  8.1 0.1 eq.81
  8.2 0.1 eq.77
  8.4 0.6 reduce-window.6
  9.0 0.2 slice_reduce_fusion
  9.3 0.1 reduce_sum.48
  9.5 0.7 and_select_fusion
  10.2 1.2 fusion.3
  11.5 1.5 fusion.1
  12.9 1.0 copy.50
  14.0 24.7 %all-to-all-start = ((bf16[32,5,16,128]{3,2,1,0:T(8,128)(2,1)}), bf16[32,5,16,128]{3,2,1,0:T(8,128)(2,1)S(1)}, u32[]{:S(2)}, u32[]{:S(2)}) async-start(bf16[32,5,16,128]{3,2,1,0:T(8,128)(2,1)} %bitcast.11), calls=%async_computation | async-start | bytes 1310720 | tf_op jit(solution)/shard_map/all_to_all | solution.py:247
  38.9 38.5 %all-to-all-done = bf16[32,5,16,128]{3,2,1,0:T(8,128)(2,1)S(1)} async-done(((bf16[32,5,16,128]{3,2,1,0:T(8,128)(2,1)}), bf16[32,5,16,128]{3,2,1,0:T(8,128)(2,1)S(1)}, u32[]{:S(2)}, u32[]{:S(2)}) %all-to-all-start) | async-done | bytes 655392 | tf_op jit(solution)/shard_map/all_to_all | solution.py:247
  77.4 0.2 copy.75
  77.6 0.2 collective-permute-start
  77.8 2.0 collective-permute-start.2
  79.8 0.4 fusion.2
  80.2 0.9 copy.53
  81.1 4.8 %all-to-all-start.2 = ((bf16[32,4,16,128]{3,2,1,0:T(8,128)(2,1)}), bf16[32,4,16,128]{3,2,1,0:T(8,128)(2,1)S(1)}, u32[]{:S(2)}, u32[]{:S(2)}) async-start(bf16[32,4,16,128]{3,2,1,0:T(8,128)(2,1)} %bitcast.20), calls=%async_computation.2 | async-start | bytes 1048576 | tf_op jit(solution)/shard_map/all_to_all | solution.py:247
  85.9 8.5 %collective-permute-done.refs_1_ = bf16[160,2048]{1,0:T(8,128)(2,1)S(1)} collective-permute-done((bf16[160,2048]{1,0:T(8,128)(2,1)S(1)}, bf16[160,2048]{1,0:T(8,128)(2,1)S(1)}, u32[]{:S(2)}, u32[]{:S(2)}) %collective-permute-start) | collective-permute-done | bytes 655392 | tf_op jit(solution)/shard_map/ppermute | solution.py:23
  94.4 1.6 collective-permute-start.1
  96.1 0.6 collective-permute-start.3
  96.7 2.0 copy-done
  98.7 2.0 copy-done.3
  100.8 2.1 copy-done.6
  102.8 9.9 %feed.4 = (bf16[160,2048]{1,0:T(8,128)(2,1)S(1)}, bf16[80,2048]{1,0:T(8,128)(2,1)S(1)}, bf16[80,2048]{1,0:T(8,128)(2,1)S(1)}, bf16[80,2048]{1,0:T(8,128)(2,1)S(1)}, bf16[80,2048]{1,0:T(8,128)(2,1)S(1)}) custom-call(bf16[160,2048]{1,0:T(8,128)(2,1)S(1)} %bitcast.61, bf16[160,2048]{1,0:T(8,128)(2,1)S(1)} %collective-permute-done.refs_1_, ...), custom_call_target="tpu_custom_call" | custom-call | flops 5284823040 | bytes 14942208 | tf_op jit(solution)/shard_map/feed/pallas_call | solution.py:158
  112.8 4.6 %feed.5 = (bf16[80,2048]{1,0:T(8,128)(2,1)S(1)}, bf16[80,2048]{1,0:T(8,128)(2,1)S(1)}) custom-call(bf16[80,2048]{1,0:T(8,128)(2,1)S(1)} %collective-permute-done.1.refs_0_, bf16[80,2048]{1,0:T(8,128)(2,1)S(1)} %collective-permute-done.3.refs_1_, bf16[1,2048,896]{2,1,0:T(8,128)(2,1)S(1)} %copy-done.1, bf16[1,2048,896]{2,1,0:T(8,128)(2,1)S(1)} %copy-done.4, ...), custom_call_target="tpu_custom_call" | custom-call | flops 1761607680 | bytes 12320768 | tf_op jit(solution)/shard_map/feed/pallas_call | solution.py:158
  117.4 0.8 collective-permute-start.8
  118.2 2.5 collective-permute-start.6
  120.8 3.2 %collective-permute-start.4 = (bf16[80,2048]{1,0:T(8,128)(2,1)S(1)}, bf16[80,2048]{1,0:T(8,128)(2,1)S(1)}, u32[]{:S(2)}, u32[]{:S(2)}) collective-permute-start(bf16[80,2048]{1,0:T(8,128)(2,1)S(1)} %get-tuple-element.29), channel_id=1, source_target_pairs={{0,1},{1,2},{2,3},{3,0},{4,5},{5,6},{6,7},{7,4},{8,9},{9,10},{10,1... | collective-permute-start | bytes 983048 | tf_op jit(solution)/shard_map/ppermute | solution.py:23
  124.0 5.3 %collective-permute-done.8 = bf16[80,2048]{1,0:T(8,128)(2,1)S(1)} collective-permute-done((bf16[80,2048]{1,0:T(8,128)(2,1)S(1)}, bf16[80,2048]{1,0:T(8,128)(2,1)S(1)}, u32[]{:S(2)}, u32[]{:S(2)}) %collective-permute-start.8) | collective-permute-done | bytes 327712 | tf_op jit(solution)/shard_map/ppermute | solution.py:23
  129.4 0.1 collective-permute-start.9
  129.5 4.1 %collective-permute-done.4 = bf16[80,2048]{1,0:T(8,128)(2,1)S(1)} collective-permute-done((bf16[80,2048]{1,0:T(8,128)(2,1)S(1)}, bf16[80,2048]{1,0:T(8,128)(2,1)S(1)}, u32[]{:S(2)}, u32[]{:S(2)}) %collective-permute-start.4) | collective-permute-done | bytes 327712 | tf_op jit(solution)/shard_map/ppermute | solution.py:23
  133.7 3.8 %collective-permute-start.5 = (bf16[80,2048]{1,0:T(8,128)(2,1)S(1)}, bf16[80,2048]{1,0:T(8,128)(2,1)S(1)}, u32[]{:S(2)}, u32[]{:S(2)}) collective-permute-start(bf16[80,2048]{1,0:T(8,128)(2,1)S(1)} %add_convert_fusion.1), channel_id=1, source_target_pairs={{0,1},{1,2},{2,3},{3,0},{4,5},{5,6},{6,7},{7,4},{8,9},{9,10},{10,1... | collective-permute-start | bytes 983048 | tf_op jit(solution)/shard_map/ppermute | solution.py:23
  137.5 3.6 %collective-permute-done.9.d_ref = bf16[80,2048]{1,0:T(8,128)(2,1)S(1)} collective-permute-done((bf16[80,2048]{1,0:T(8,128)(2,1)S(1)}, bf16[80,2048]{1,0:T(8,128)(2,1)S(1)}, u32[]{:S(2)}, u32[]{:S(2)}) %collective-permute-start.9) | collective-permute-done | bytes 327712 | tf_op jit(solution)/shard_map/ppermute | solution.py:23
  141.1 1.4 collective-permute-done.5.a_ref
  142.5 1.7 join.2
  144.2 5.0 %all-to-all-start.1 = ((bf16[32,5,16,128]{3,2,1,0:T(8,128)(2,1)}), bf16[32,5,16,128]{3,2,1,0:T(8,128)(2,1)S(1)}, u32[]{:S(2)}, u32[]{:S(2)}) async-start(bf16[32,5,16,128]{3,2,1,0:T(8,128)(2,1)} %bitcast.5), calls=%async_computation.1 | async-start | bytes 1310720 | tf_op jit(solution)/shard_map/all_to_all | solution.py:247
  149.2 0.1 copy.76
  149.4 3.8 %collective-permute-start.10 = (bf16[128,2048]{1,0:T(8,128)(2,1)S(1)}, bf16[128,2048]{1,0:T(8,128)(2,1)S(1)}, u32[]{:S(2)}, u32[]{:S(2)}) collective-permute-start(bf16[128,2048]{1,0:T(8,128)(2,1)S(1)} %bitcast.62), channel_id=1, source_target_pairs={{0,1},{1,2},{2,3},{3,0},{4,5},{5,6},{6,7},{7,4},{8,9},{9,10},{10,1... | collective-permute-start | bytes 1572872 | tf_op jit(solution)/shard_map/ppermute | solution.py:23
  153.2 11.2 %collective-permute-done.10.refs_1_ = bf16[128,2048]{1,0:T(8,128)(2,1)S(1)} collective-permute-done((bf16[128,2048]{1,0:T(8,128)(2,1)S(1)}, bf16[128,2048]{1,0:T(8,128)(2,1)S(1)}, u32[]{:S(2)}, u32[]{:S(2)}) %collective-permute-start.10) | collective-permute-done | bytes 524320 | tf_op jit(solution)/shard_map/ppermute | solution.py:23
  164.4 3.8 %collective-permute-start.11 = (bf16[64,2048]{1,0:T(8,128)(2,1)S(1)}, bf16[64,2048]{1,0:T(8,128)(2,1)S(1)}, u32[]{:S(2)}, u32[]{:S(2)}) collective-permute-start(bf16[64,2048]{1,0:T(8,128)(2,1)S(1)} %slice.43), channel_id=1, source_target_pairs={{0,1},{1,2},{2,3},{3,0},{4,5},{5,6},{6,7},{7,4},{8,9},{9,10},{10,1... | collective-permute-start | bytes 786440 | tf_op jit(solution)/shard_map/ppermute | solution.py:23
  168.2 0.1 collective-permute-start.13
  168.4 2.0 copy-done.2
  170.4 2.0 copy-done.5
  172.4 2.0 copy-done.8
  174.5 8.3 %feed.6 = (bf16[128,2048]{1,0:T(8,128)(2,1)S(1)}, bf16[64,2048]{1,0:T(8,128)(2,1)S(1)}, bf16[64,2048]{1,0:T(8,128)(2,1)S(1)}, bf16[64,2048]{1,0:T(8,128)(2,1)S(1)}, bf16[64,2048]{1,0:T(8,128)(2,1)S(1)}) custom-call(bf16[128,2048]{1,0:T(8,128)(2,1)S(1)} %bitcast.64, bf16[128,2048]{1,0:T(8,128)(2,1)S(1)} %collective-permute-done.10.refs_1_, ...), custom_call_target="tpu_custom_call" | custom-call | flops 4227858432 | bytes 14155776 | tf_op jit(solution)/shard_map/feed/pallas_call | solution.py:158
  182.8 4.1 %feed.7 = (bf16[64,2048]{1,0:T(8,128)(2,1)S(1)}, bf16[64,2048]{1,0:T(8,128)(2,1)S(1)}) custom-call(bf16[64,2048]{1,0:T(8,128)(2,1)S(1)} %collective-permute-done.11.refs_0_, bf16[64,2048]{1,0:T(8,128)(2,1)S(1)} %collective-permute-done.13.refs_1_, bf16[1,2048,896]{2,1,0:T(8,128)(2,1)S(1)} %copy-done.2, bf16[1,2048,896]{2,1,0:T(8,128)(2,1)S(1)} %copy-done.5, ...), custom_call_target="tpu_custom_call" | custom-call | flops 1409286144 | bytes 12058624 | tf_op jit(solution)/shard_map/feed/pallas_call | solution.py:158
  186.9 0.1 collective-permute-start.18
  187.1 3.5 %collective-permute-start.16 = (bf16[64,2048]{1,0:T(8,128)(2,1)S(1)}, bf16[64,2048]{1,0:T(8,128)(2,1)S(1)}, u32[]{:S(2)}, u32[]{:S(2)}) collective-permute-start(bf16[64,2048]{1,0:T(8,128)(2,1)S(1)} %get-tuple-element.40), channel_id=1, source_target_pairs={{0,1},{1,2},{2,3},{3,0},{4,5},{5,6},{6,7},{7,4},{8,9},{9,10},{10,1... | collective-permute-start | bytes 786440 | tf_op jit(solution)/shard_map/ppermute | solution.py:23
  190.6 3.2 %collective-permute-start.14 = (bf16[64,2048]{1,0:T(8,128)(2,1)S(1)}, bf16[64,2048]{1,0:T(8,128)(2,1)S(1)}, u32[]{:S(2)}, u32[]{:S(2)}) collective-permute-start(bf16[64,2048]{1,0:T(8,128)(2,1)S(1)} %get-tuple-element.39), channel_id=1, source_target_pairs={{0,1},{1,2},{2,3},{3,0},{4,5},{5,6},{6,7},{7,4},{8,9},{9,10},{10,1... | collective-permute-start | bytes 786440 | tf_op jit(solution)/shard_map/ppermute | solution.py:23
  193.8 3.6 %collective-permute-done.18 = bf16[64,2048]{1,0:T(8,128)(2,1)S(1)} collective-permute-done((bf16[64,2048]{1,0:T(8,128)(2,1)S(1)}, bf16[64,2048]{1,0:T(8,128)(2,1)S(1)}, u32[]{:S(2)}, u32[]{:S(2)}) %collective-permute-start.18) | collective-permute-done | bytes 262176 | tf_op jit(solution)/shard_map/ppermute | solution.py:23
  197.6 2.7 %collective-permute-done.14 = bf16[64,2048]{1,0:T(8,128)(2,1)S(1)} collective-permute-done((bf16[64,2048]{1,0:T(8,128)(2,1)S(1)}, bf16[64,2048]{1,0:T(8,128)(2,1)S(1)}, u32[]{:S(2)}, u32[]{:S(2)}) %collective-permute-start.14) | collective-permute-done | bytes 262176 | tf_op jit(solution)/shard_map/ppermute | solution.py:23
  200.4 3.8 %collective-permute-start.15 = (bf16[64,2048]{1,0:T(8,128)(2,1)S(1)}, bf16[64,2048]{1,0:T(8,128)(2,1)S(1)}, u32[]{:S(2)}, u32[]{:S(2)}) collective-permute-start(bf16[64,2048]{1,0:T(8,128)(2,1)S(1)} %add_convert_fusion.3), channel_id=1, source_target_pairs={{0,1},{1,2},{2,3},{3,0},{4,5},{5,6},{6,7},{7,4},{8,9},{9,10},{10,1... | collective-permute-start | bytes 786440 | tf_op jit(solution)/shard_map/ppermute | solution.py:23
  204.2 2.1 collective-permute-done.19.d_ref
  206.4 1.7 collective-permute-done.15.a_ref
  208.1 1.4 join.3
  209.5 13.0 %all-to-all-start.3 = ((bf16[32,4,16,128]{3,2,1,0:T(8,128)(2,1)}), bf16[32,4,16,128]{3,2,1,0:T(8,128)(2,1)S(1)}, u32[]{:S(2)}, u32[]{:S(2)}) async-start(bf16[32,4,16,128]{3,2,1,0:T(8,128)(2,1)} %bitcast.6), calls=%async_computation.3 | async-start | bytes 1048576 | tf_op jit(solution)/shard_map/all_to_all | solution.py:247
  222.8 0.3 fusion.7
  223.2 0.3 convolution_add_fusion.2
  223.5 32.2 %all-to-all-done.3 = bf16[32,4,16,128]{3,2,1,0:T(8,128)(2,1)S(1)} async-done(((bf16[32,4,16,128]{3,2,1,0:T(8,128)(2,1)}), bf16[32,4,16,128]{3,2,1,0:T(8,128)(2,1)S(1)}, u32[]{:S(2)}, u32[]{:S(2)}) %all-to-all-start.3) | async-done | bytes 524320 | tf_op jit(solution)/shard_map/all_to_all | solution.py:247
  255.7 0.3 convolution_add_fusion.1
  256.0 1.1 fusion
  257.1 2.2 copy-done.9
  259.3 2.4 mixer.1
  (76 shorter events, 1.2 us)
Async XLA Ops:
  7.2 72.6 %copy-start.12 = (bf16[128,2048]{1,0:T(8,128)(2,1)S(1)}, bf16[128,2048]{1,0:T(8,128)(2,1)}, u32[]{:S(2)}) copy-start(bf16[128,2048]{1,0:T(8,128)(2,1)} %param.17) | copy-start | bytes 1572868
  7.2 72.6 %copy-start.16 = (f32[2048]{0:T(1024)S(1)}, f32[2048]{0:T(1024)}, u32[]{:S(2)}) copy-start(f32[2048]{0:T(1024)} %param.20) | copy-start | bytes 24580
  7.2 31.6 %copy-start.14 = (bf16[128,256]{1,0:T(8,128)(2,1)S(1)}, bf16[128,256]{1,0:T(8,128)(2,1)}, u32[]{:S(2)}) copy-start(bf16[128,256]{1,0:T(8,128)(2,1)} %param.13) | copy-start | bytes 196612
  7.2 31.6 %copy-start.15 = (bf16[128,256]{1,0:T(8,128)(2,1)S(1)}, bf16[128,256]{1,0:T(8,128)(2,1)}, u32[]{:S(2)}) copy-start(bf16[128,256]{1,0:T(8,128)(2,1)} %param.14) | copy-start | bytes 196612
  7.2 31.6 %copy-start.18 = (bf16[128,2]{0,1:T(2,128)(2,1)S(1)}, bf16[128,2]{0,1:T(2,128)(2,1)}, u32[]{:S(2)}) copy-start(bf16[128,2]{0,1:T(2,128)(2,1)} %param.15) | copy-start | bytes 1540
  14.0 63.4 %all-to-all-start = ((bf16[32,5,16,128]{3,2,1,0:T(8,128)(2,1)}), bf16[32,5,16,128]{3,2,1,0:T(8,128)(2,1)S(1)}, u32[]{:S(2)}, u32[]{:S(2)}) async-start(bf16[32,5,16,128]{3,2,1,0:T(8,128)(2,1)} %bitcast.11), calls=%async_computation | async-start | bytes 1310720 | tf_op jit(solution)/shard_map/all_to_all | solution.py:247
  38.7 218.3 %all-gather.2.cloned.1.call-start = ((), (), s32[]{:S(2)}) async-start(), calls=%async_computation.4 | async-start | bytes 4392960 | tf_op jit(solution)/shard_map/all_gather | solution.py:303
  38.9 38.7 %copy-start.13 = (bf16[520,128]{1,0:T(8,128)(2,1)}, bf16[520,128]{1,0:T(8,128)(2,1)S(1)}, u32[]{:S(2)}) copy-start(bf16[520,128]{1,0:T(8,128)(2,1)S(1)} %constant_dynamic-update-slice_fusion) | copy-start | bytes 399364
  77.6 16.8 %collective-permute-start = (bf16[160,2048]{1,0:T(8,128)(2,1)S(1)}, bf16[160,2048]{1,0:T(8,128)(2,1)S(1)}, u32[]{:S(2)}, u32[]{:S(2)}) collective-permute-start(bf16[160,2048]{1,0:T(8,128)(2,1)S(1)} %bitcast.59), channel_id=1, source_target_pairs={{0,1},{1,2},{2,3},{3,0},{4,5},{5,6},{6,7},{7,4},{8,9},{9,10},{10,1... | collective-permute-start | bytes 1966088 | tf_op jit(solution)/shard_map/ppermute | solution.py:23
  77.8 18.2 %collective-permute-start.2 = (bf16[160,2048]{1,0:T(8,128)(2,1)S(1)}, bf16[160,2048]{1,0:T(8,128)(2,1)S(1)}, u32[]{:S(2)}, u32[]{:S(2)}) collective-permute-start(bf16[160,2048]{1,0:T(8,128)(2,1)S(1)} %bitcast.60), channel_id=1, source_target_pairs={{0,3},{1,0},{2,1},{3,2},{4,7},{5,4},{6,5},{7,6},{8,11},{9,8},{10,9... | collective-permute-start | bytes 1966088 | tf_op jit(solution)/shard_map/ppermute | solution.py:23
  81.1 63.1 %all-to-all-start.2 = ((bf16[32,4,16,128]{3,2,1,0:T(8,128)(2,1)}), bf16[32,4,16,128]{3,2,1,0:T(8,128)(2,1)S(1)}, u32[]{:S(2)}, u32[]{:S(2)}) async-start(bf16[32,4,16,128]{3,2,1,0:T(8,128)(2,1)} %bitcast.20), calls=%async_computation.2 | async-start | bytes 1048576 | tf_op jit(solution)/shard_map/all_to_all | solution.py:247
  94.4 18.3 %collective-permute-start.1 = (bf16[80,2048]{1,0:T(8,128)(2,1)S(1)}, bf16[80,2048]{1,0:T(8,128)(2,1)S(1)}, u32[]{:S(2)}, u32[]{:S(2)}) collective-permute-start(bf16[80,2048]{1,0:T(8,128)(2,1)S(1)} %slice.41), channel_id=1, source_target_pairs={{0,1},{1,2},{2,3},{3,0},{4,5},{5,6},{6,7},{7,4},{8,9},{9,10},{10,1... | collective-permute-start | bytes 983048 | tf_op jit(solution)/shard_map/ppermute | solution.py:23
  96.1 16.6 %collective-permute-start.3 = (bf16[80,2048]{1,0:T(8,128)(2,1)S(1)}, bf16[80,2048]{1,0:T(8,128)(2,1)S(1)}, u32[]{:S(2)}, u32[]{:S(2)}) collective-permute-start(bf16[80,2048]{1,0:T(8,128)(2,1)S(1)} %slice.42), channel_id=1, source_target_pairs={{0,3},{1,0},{2,1},{3,2},{4,7},{5,4},{6,5},{7,6},{8,11},{9,8},{10,9... | collective-permute-start | bytes 983048 | tf_op jit(solution)/shard_map/ppermute | solution.py:23
  96.7 2.0 copy-start
  98.7 2.0 copy-start.3
  100.8 2.1 copy-start.6
  102.8 9.9 %copy-start.1 = (bf16[1,2048,896]{2,1,0:T(8,128)(2,1)S(1)}, bf16[1,2048,896]{2,1,0:T(8,128)(2,1)}, u32[]{:S(2)}) copy-start(bf16[1,2048,896]{2,1,0:T(8,128)(2,1)} %refs_2_.3) | copy-start | bytes 11010052
  102.8 9.9 %copy-start.4 = (bf16[1,2048,896]{2,1,0:T(8,128)(2,1)S(1)}, bf16[1,2048,896]{2,1,0:T(8,128)(2,1)}, u32[]{:S(2)}) copy-start(bf16[1,2048,896]{2,1,0:T(8,128)(2,1)} %refs_3_.7) | copy-start | bytes 11010052
  102.8 9.9 %copy-start.7 = (bf16[1,896,2048]{2,1,0:T(8,128)(2,1)S(1)}, bf16[1,896,2048]{2,1,0:T(8,128)(2,1)}, u32[]{:S(2)}) copy-start(bf16[1,896,2048]{2,1,0:T(8,128)(2,1)} %refs_4_.7) | copy-start | bytes 11010052
  117.4 11.9 %collective-permute-start.8 = (bf16[80,2048]{1,0:T(8,128)(2,1)S(1)}, bf16[80,2048]{1,0:T(8,128)(2,1)S(1)}, u32[]{:S(2)}, u32[]{:S(2)}) collective-permute-start(bf16[80,2048]{1,0:T(8,128)(2,1)S(1)} %get-tuple-element.33), channel_id=1, source_target_pairs={{0,3},{1,0},{2,1},{3,2},{4,7},{5,4},{6,5},{7,6},{8,11},{9,8},{10,9... | collective-permute-start | bytes 983048 | tf_op jit(solution)/shard_map/ppermute | solution.py:23
  118.2 19.3 %collective-permute-start.6 = (bf16[80,2048]{1,0:T(8,128)(2,1)S(1)}, bf16[80,2048]{1,0:T(8,128)(2,1)S(1)}, u32[]{:S(2)}, u32[]{:S(2)}) collective-permute-start(bf16[80,2048]{1,0:T(8,128)(2,1)S(1)} %get-tuple-element.30), channel_id=1, source_target_pairs={{0,1},{1,2},{2,3},{3,0},{4,5},{5,6},{6,7},{7,4},{8,9},{9,10},{10,1... | collective-permute-start | bytes 983048 | tf_op jit(solution)/shard_map/ppermute | solution.py:23
  120.8 16.8 %collective-permute-start.7 = (bf16[80,2048]{1,0:T(8,128)(2,1)S(1)}, bf16[80,2048]{1,0:T(8,128)(2,1)S(1)}, u32[]{:S(2)}, u32[]{:S(2)}) collective-permute-start(bf16[80,2048]{1,0:T(8,128)(2,1)S(1)} %get-tuple-element.31), channel_id=1, source_target_pairs={{0,3},{1,0},{2,1},{3,2},{4,7},{5,4},{6,5},{7,6},{8,11},{9,8},{10,9... | collective-permute-start | bytes 983048 | tf_op jit(solution)/shard_map/ppermute | solution.py:23
  120.8 12.9 %collective-permute-start.4 = (bf16[80,2048]{1,0:T(8,128)(2,1)S(1)}, bf16[80,2048]{1,0:T(8,128)(2,1)S(1)}, u32[]{:S(2)}, u32[]{:S(2)}) collective-permute-start(bf16[80,2048]{1,0:T(8,128)(2,1)S(1)} %get-tuple-element.29), channel_id=1, source_target_pairs={{0,1},{1,2},{2,3},{3,0},{4,5},{5,6},{6,7},{7,4},{8,9},{9,10},{10,1... | collective-permute-start | bytes 983048 | tf_op jit(solution)/shard_map/ppermute | solution.py:23
  129.4 11.7 %collective-permute-start.9 = (bf16[80,2048]{1,0:T(8,128)(2,1)S(1)}, bf16[80,2048]{1,0:T(8,128)(2,1)S(1)}, u32[]{:S(2)}, u32[]{:S(2)}) collective-permute-start(bf16[80,2048]{1,0:T(8,128)(2,1)S(1)} %add_convert_fusion), channel_id=1, source_target_pairs={{0,3},{1,0},{2,1},{3,2},{4,7},{5,4},{6,5},{7,6},{8,11},{9,8},{10,9... | collective-permute-start | bytes 983048 | tf_op jit(solution)/shard_map/ppermute | solution.py:23
  133.7 8.8 %collective-permute-start.5 = (bf16[80,2048]{1,0:T(8,128)(2,1)S(1)}, bf16[80,2048]{1,0:T(8,128)(2,1)S(1)}, u32[]{:S(2)}, u32[]{:S(2)}) collective-permute-start(bf16[80,2048]{1,0:T(8,128)(2,1)S(1)} %add_convert_fusion.1), channel_id=1, source_target_pairs={{0,1},{1,2},{2,3},{3,0},{4,5},{5,6},{6,7},{7,4},{8,9},{9,10},{10,1... | collective-permute-start | bytes 983048 | tf_op jit(solution)/shard_map/ppermute | solution.py:23
  144.2 65.3 %all-to-all-start.1 = ((bf16[32,5,16,128]{3,2,1,0:T(8,128)(2,1)}), bf16[32,5,16,128]{3,2,1,0:T(8,128)(2,1)S(1)}, u32[]{:S(2)}, u32[]{:S(2)}) async-start(bf16[32,5,16,128]{3,2,1,0:T(8,128)(2,1)} %bitcast.5), calls=%async_computation.1 | async-start | bytes 1310720 | tf_op jit(solution)/shard_map/all_to_all | solution.py:247
  149.4 15.0 %collective-permute-start.10 = (bf16[128,2048]{1,0:T(8,128)(2,1)S(1)}, bf16[128,2048]{1,0:T(8,128)(2,1)S(1)}, u32[]{:S(2)}, u32[]{:S(2)}) collective-permute-start(bf16[128,2048]{1,0:T(8,128)(2,1)S(1)} %bitcast.62), channel_id=1, source_target_pairs={{0,1},{1,2},{2,3},{3,0},{4,5},{5,6},{6,7},{7,4},{8,9},{9,10},{10,1... | collective-permute-start | bytes 1572872 | tf_op jit(solution)/shard_map/ppermute | solution.py:23
  153.2 15.0 %collective-permute-start.12 = (bf16[128,2048]{1,0:T(8,128)(2,1)S(1)}, bf16[128,2048]{1,0:T(8,128)(2,1)S(1)}, u32[]{:S(2)}, u32[]{:S(2)}) collective-permute-start(bf16[128,2048]{1,0:T(8,128)(2,1)S(1)} %bitcast.63), channel_id=1, source_target_pairs={{0,3},{1,0},{2,1},{3,2},{4,7},{5,4},{6,5},{7,6},{8,11},{9,8},{10,9... | collective-permute-start | bytes 1572872 | tf_op jit(solution)/shard_map/ppermute | solution.py:23
  164.4 18.4 %collective-permute-start.11 = (bf16[64,2048]{1,0:T(8,128)(2,1)S(1)}, bf16[64,2048]{1,0:T(8,128)(2,1)S(1)}, u32[]{:S(2)}, u32[]{:S(2)}) collective-permute-start(bf16[64,2048]{1,0:T(8,128)(2,1)S(1)} %slice.43), channel_id=1, source_target_pairs={{0,1},{1,2},{2,3},{3,0},{4,5},{5,6},{6,7},{7,4},{8,9},{9,10},{10,1... | collective-permute-start | bytes 786440 | tf_op jit(solution)/shard_map/ppermute | solution.py:23
  168.2 14.6 %collective-permute-start.13 = (bf16[64,2048]{1,0:T(8,128)(2,1)S(1)}, bf16[64,2048]{1,0:T(8,128)(2,1)S(1)}, u32[]{:S(2)}, u32[]{:S(2)}) collective-permute-start(bf16[64,2048]{1,0:T(8,128)(2,1)S(1)} %slice.44), channel_id=1, source_target_pairs={{0,3},{1,0},{2,1},{3,2},{4,7},{5,4},{6,5},{7,6},{8,11},{9,8},{10,9... | collective-permute-start | bytes 786440 | tf_op jit(solution)/shard_map/ppermute | solution.py:23
  168.3 2.0 copy-start.2
  170.4 2.0 copy-start.5
  172.4 2.0 copy-start.8
  186.9 35.7 %copy-start.17 = (f32[128,2]{0,1:T(2,128)S(1)}, f32[128,2]{0,1:T(2,128)}, u32[]{:S(2)}) copy-start(f32[128,2]{0,1:T(2,128)} %param.19) | copy-start | bytes 3076
  186.9 10.5 %collective-permute-start.18 = (bf16[64,2048]{1,0:T(8,128)(2,1)S(1)}, bf16[64,2048]{1,0:T(8,128)(2,1)S(1)}, u32[]{:S(2)}, u32[]{:S(2)}) collective-permute-start(bf16[64,2048]{1,0:T(8,128)(2,1)S(1)} %get-tuple-element.43), channel_id=1, source_target_pairs={{0,3},{1,0},{2,1},{3,2},{4,7},{5,4},{6,5},{7,6},{8,11},{9,8},{10,9... | collective-permute-start | bytes 786440 | tf_op jit(solution)/shard_map/ppermute | solution.py:23
  187.1 17.2 %collective-permute-start.16 = (bf16[64,2048]{1,0:T(8,128)(2,1)S(1)}, bf16[64,2048]{1,0:T(8,128)(2,1)S(1)}, u32[]{:S(2)}, u32[]{:S(2)}) collective-permute-start(bf16[64,2048]{1,0:T(8,128)(2,1)S(1)} %get-tuple-element.40), channel_id=1, source_target_pairs={{0,1},{1,2},{2,3},{3,0},{4,5},{5,6},{6,7},{7,4},{8,9},{9,10},{10,1... | collective-permute-start | bytes 786440 | tf_op jit(solution)/shard_map/ppermute | solution.py:23
  190.6 13.6 %collective-permute-start.17 = (bf16[64,2048]{1,0:T(8,128)(2,1)S(1)}, bf16[64,2048]{1,0:T(8,128)(2,1)S(1)}, u32[]{:S(2)}, u32[]{:S(2)}) collective-permute-start(bf16[64,2048]{1,0:T(8,128)(2,1)S(1)} %get-tuple-element.41), channel_id=1, source_target_pairs={{0,3},{1,0},{2,1},{3,2},{4,7},{5,4},{6,5},{7,6},{8,11},{9,8},{10,9... | collective-permute-start | bytes 786440 | tf_op jit(solution)/shard_map/ppermute | solution.py:23
  190.6 9.7 %collective-permute-start.14 = (bf16[64,2048]{1,0:T(8,128)(2,1)S(1)}, bf16[64,2048]{1,0:T(8,128)(2,1)S(1)}, u32[]{:S(2)}, u32[]{:S(2)}) collective-permute-start(bf16[64,2048]{1,0:T(8,128)(2,1)S(1)} %get-tuple-element.39), channel_id=1, source_target_pairs={{0,1},{1,2},{2,3},{3,0},{4,5},{5,6},{6,7},{7,4},{8,9},{9,10},{10,1... | collective-permute-start | bytes 786440 | tf_op jit(solution)/shard_map/ppermute | solution.py:23
  197.5 8.9 %collective-permute-start.19 = (bf16[64,2048]{1,0:T(8,128)(2,1)S(1)}, bf16[64,2048]{1,0:T(8,128)(2,1)S(1)}, u32[]{:S(2)}, u32[]{:S(2)}) collective-permute-start(bf16[64,2048]{1,0:T(8,128)(2,1)S(1)} %add_convert_fusion.2), channel_id=1, source_target_pairs={{0,3},{1,0},{2,1},{3,2},{4,7},{5,4},{6,5},{7,6},{8,11},{9,8},{10,9... | collective-permute-start | bytes 786440 | tf_op jit(solution)/shard_map/ppermute | solution.py:23
  200.4 7.7 %collective-permute-start.15 = (bf16[64,2048]{1,0:T(8,128)(2,1)S(1)}, bf16[64,2048]{1,0:T(8,128)(2,1)S(1)}, u32[]{:S(2)}, u32[]{:S(2)}) collective-permute-start(bf16[64,2048]{1,0:T(8,128)(2,1)S(1)} %add_convert_fusion.3), channel_id=1, source_target_pairs={{0,1},{1,2},{2,3},{3,0},{4,5},{5,6},{6,7},{7,4},{8,9},{9,10},{10,1... | collective-permute-start | bytes 786440 | tf_op jit(solution)/shard_map/ppermute | solution.py:23
  209.5 46.1 %all-to-all-start.3 = ((bf16[32,4,16,128]{3,2,1,0:T(8,128)(2,1)}), bf16[32,4,16,128]{3,2,1,0:T(8,128)(2,1)S(1)}, u32[]{:S(2)}, u32[]{:S(2)}) async-start(bf16[32,4,16,128]{3,2,1,0:T(8,128)(2,1)} %bitcast.6), calls=%async_computation.3 | async-start | bytes 1048576 | tf_op jit(solution)/shard_map/all_to_all | solution.py:247
  223.1 33.9 %copy-start.10 = (bf16[128,256]{1,0:T(8,128)(2,1)S(1)}, bf16[128,256]{1,0:T(8,128)(2,1)}, u32[]{:S(2)}) copy-start(bf16[128,256]{1,0:T(8,128)(2,1)} %q_ref.1) | copy-start | bytes 196612
  223.1 33.9 %copy-start.11 = (f32[256]{0:T(256)S(1)}, f32[256]{0:T(256)}, u32[]{:S(2)}) copy-start(f32[256]{0:T(256)} %param.16) | copy-start | bytes 3076
  257.1 2.2 copy-start.9
Sparse Core Ops, SparseCore 0:
  77.8 81.5 all-gather.1
